TPU v7x, 32 devices: a whole 2x2x4 slice. The times are simulated.
32 devices in a mesh: fs: 16 (over z, y, x), tp: 2 (over core).
Axes of the slice: x: 2, y: 2, z: 4, core: 2. Of those that a mesh axis runs over, the one named last changes fastest.
Arguments:
- saved_inputs: bfloat16 [12288, 2048], P('fs'), may hold values from -8 to 8
- input_cot: bfloat16 [12288, 2048], P('fs', 'tp'), may hold values from -0.0546875 to 0.0546875
- gate_cot: bfloat16 [12288, 2048], P('fs', 'tp'), may hold values from -0.0546875 to 0.0546875
- input_master: float32 [2048, 2048], P('fs', 'tp'), may hold values from -6 to 6
- gate_master: float32 [2048, 2048], P('fs', 'tp'), may hold values from -6 to 6
- input_factor: bfloat16 [2048, 256], P('fs'), may hold values from -2 to 2
- gate_factor: bfloat16 [2048, 256], P('fs'), may hold values from -2 to 2
- input_first: float32 [256, 2048], P('fs', 'tp'), may hold values from -6 to 6
- input_second: float32 [256, 2048], P('fs', 'tp'), may hold values from 0.2 to 17
- gate_first: float32 [256, 2048], P('fs', 'tp'), may hold values from -6 to 6
- gate_second: float32 [256, 2048], P('fs', 'tp'), may hold values from 0.2 to 17
Outputs:
- input_step: float32 [2048, 2048], P('fs', 'tp')
- gate_step: float32 [2048, 2048], P('fs', 'tp')
- input_first_new: float32 [256, 2048], P('fs', 'tp')
- input_second_new: float32 [256, 2048], P('fs', 'tp')
- gate_first_new: float32 [256, 2048], P('fs', 'tp')
- gate_second_new: float32 [256, 2048], P('fs', 'tp')
- input_copy: bfloat16 [2048, 2048], P(None, 'tp')
- gate_copy: bfloat16 [2048, 2048], P(None, 'tp')
All inputs are finite; a program needn't handle non-finite values.
Results may differ from a plain program's by a relative error of at most 0.0004.
Values may be sent and summed in bfloat16 or wider, within the bound.
A program may use at most 64 MiB of HBM per device.

v0:
```python
import jax
import jax.numpy as jnp
from jax import lax
from jax.sharding import PartitionSpec as P

D = 2048
W = 2048


first_decay = 0.9
second_decay = 0.9
ratio_floor = 1e-08
mean_floor = 1e-06
step_size = 0.05


def moments(low_rank, first, second):
    first_new = first_decay * first + (1.0 - first_decay) * low_rank
    second_new = second_decay * second + (1.0 - second_decay) * low_rank * low_rank
    ratio = first_new / (jnp.sqrt(second_new) + ratio_floor)
    return (first_new, second_new, ratio)


def local(
    saved_inputs,
    input_cot,
    gate_cot,
    input_master,
    gate_master,
    input_factor,
    gate_factor,
    input_first,
    input_second,
    gate_first,
    gate_second,
):
    col_width = input_cot.shape[1]
    contract = (((0,), (0,)), ((), ()))
    factor_in = input_factor.astype(jnp.float32)
    factor_gate = gate_factor.astype(jnp.float32)
    whole_in, whole_gate = (
        lax.all_gather(input_factor, "fs", axis=0, tiled=True),
        lax.all_gather(gate_factor, "fs", axis=0, tiled=True),
    )
    partial_in = lax.dot_general(
        saved_inputs, input_cot, contract, preferred_element_type=jnp.float32
    )
    partial_gate = lax.dot_general(
        saved_inputs, gate_cot, contract, preferred_element_type=jnp.float32
    )
    cols_in = whole_in.astype(jnp.float32)
    cols_gate = whole_gate.astype(jnp.float32)
    term_in = lax.dot_general(cols_in, partial_in, contract, precision=lax.Precision.HIGHEST)
    term_gate = lax.dot_general(cols_gate, partial_gate, contract, precision=lax.Precision.HIGHEST)
    summed = lax.psum_scatter(
        jnp.concatenate([term_in, term_gate], axis=1), "fs", scatter_dimension=0, tiled=True
    )
    low_in = summed[:, :col_width]
    low_gate = summed[:, col_width:]
    first_in, second_in, ratio_in = moments(low_in, input_first, input_second)
    first_gate, second_gate, ratio_gate = moments(low_gate, gate_first, gate_second)
    piece_in = lax.all_gather(ratio_in, "fs", axis=0, tiled=True)
    piece_gate = lax.all_gather(ratio_gate, "fs", axis=0, tiled=True)
    cols_in = factor_in
    cols_gate = factor_gate
    dir_in = jnp.dot(cols_in, piece_in, precision=lax.Precision.HIGHEST)
    dir_gate = jnp.dot(cols_gate, piece_gate, precision=lax.Precision.HIGHEST)
    square_in, square_gate = lax.psum(
        (jnp.sum(dir_in * dir_in), jnp.sum(dir_gate * dir_gate)), ("fs", "tp")
    )
    step_in = dir_in * lax.rsqrt(square_in / (D * W) + mean_floor)
    step_gate = dir_gate * lax.rsqrt(square_gate / (D * W) + mean_floor)
    local_in = (input_master - step_size * step_in).astype(jnp.bfloat16)
    local_gate = (gate_master - step_size * step_gate).astype(jnp.bfloat16)
    copy_in, copy_gate = (
        lax.all_gather(local_in, "fs", axis=0, tiled=True),
        lax.all_gather(local_gate, "fs", axis=0, tiled=True),
    )
    return (step_in, step_gate, first_in, second_in, first_gate, second_gate, copy_in, copy_gate)


def solution(mesh):
    return jax.shard_map(
        local,
        mesh=mesh,
        in_specs=(
            P("fs", None),
            P("fs", "tp"),
            P("fs", "tp"),
            P("fs", "tp"),
            P("fs", "tp"),
            P("fs", None),
            P("fs", None),
            P("fs", "tp"),
            P("fs", "tp"),
            P("fs", "tp"),
            P("fs", "tp"),
        ),
        out_specs=(
            P("fs", "tp"),
            P("fs", "tp"),
            P("fs", "tp"),
            P("fs", "tp"),
            P("fs", "tp"),
            P("fs", "tp"),
            P(None, "tp"),
            P(None, "tp"),
        ),
        check_vma=False,
    )
```

profile of v0, /device:TPU:0, one launch (start us, length us, event | category | flops | bytes accessed | tf_op | source)
XLA Modules:
  0.0 569.3 jit_solution(10387800890137530023)
XLA Ops:
  7.2 0.0 copy-start
  7.2 0.0 all-gather.7.cloned.1.call-start
  7.2 0.7 all-gather.7.cloned.1.call-update
  7.9 0.0 all-gather.9.cloned.1.call-start
  8.0 0.7 all-gather.9.cloned.1.call-update
  8.7 0.0 reduce-scatter.4.cloned.1.call-start
  8.7 0.3 copy-done
  9.1 7.2 %fusion.4 = f32[2048,1024]{1,0:T(8,128)} fusion(bf16[768,2048]{1,0:T(8,128)(2,1)S(1)} %copy-done, bf16[768,1024]{1,0:T(8,128)(2,1)} %param.12), kind=kOutput, calls=%fused_computation.17 | convolution fusion | flops 3221225472 | bytes 13107200 | tf_op jit(solution)/shard_map/dot_general | solution.py:45
  16.2 0.0 copy-done.8
  16.2 5.7 %fusion.5 = f32[2048,1024]{1,0:T(8,128)} fusion(bf16[768,2048]{1,0:T(8,128)(2,1)S(1)} %copy-done, bf16[768,1024]{1,0:T(8,128)(2,1)S(1)} %copy-done.8), kind=kOutput, calls=%fused_computation.18 | convolution fusion | flops 3221225472 | bytes 13107200 | tf_op jit(solution)/shard_map/dot_general | solution.py:48
  21.9 46.7 %all-gather.7.cloned.1.call-done = bf16[2048,256]{1,0:T(8,128)(2,1)} async-done(((bf16[128,256]{1,0:T(8,128)(2,1)}), bf16[2048,256]{1,0:T(8,128)(2,1)}) %all-gather.7.cloned.1.call-update) | async-done | bytes 1048592 | tf_op jit(solution)/shard_map/all_gather | solution.py:42
  68.6 11.2 %convolution_bitcast_fusion.1 = f32[256,1024]{0,1:T(8,128)} fusion(f32[2048,1024]{1,0:T(8,128)} %fusion.4, bf16[2048,256]{1,0:T(8,128)(2,1)} %all-gather.7.cloned.1.call-done), kind=kOutput, calls=%fused_computation.2 | convolution fusion | flops 6442450944 | bytes 10485760 | tf_op jit(solution)/shard_map/dot_general | solution.py:53
  79.8 45.5 %all-gather.9.cloned.1.call-done = bf16[2048,256]{1,0:T(8,128)(2,1)} async-done(((bf16[128,256]{1,0:T(8,128)(2,1)}), bf16[2048,256]{1,0:T(8,128)(2,1)}) %all-gather.9.cloned.1.call-update) | async-done | bytes 1048592 | tf_op jit(solution)/shard_map/all_gather | solution.py:43
  125.3 9.5 %convolution_bitcast_fusion = f32[256,1024]{0,1:T(8,128)S(1)} fusion(f32[2048,1024]{1,0:T(8,128)} %fusion.5, bf16[2048,256]{1,0:T(8,128)(2,1)} %all-gather.9.cloned.1.call-done), kind=kOutput, calls=%fused_computation.1 | convolution fusion | flops 6442450944 | bytes 10485760 | tf_op jit(solution)/shard_map/dot_general | solution.py:54
  134.8 0.0 copy-done.1
  134.8 1.5 pad_maximum_fusion
  136.2 0.0 copy-start.2
  136.3 2.9 copy.65
  139.2 0.0 reduce-scatter.4.cloned.1.call-update
  139.2 0.0 all-gather.13.cloned.1.call-start
  139.3 80.6 %reduce-scatter.4.cloned.1.call-done = f32[16,2048]{1,0:T(8,128)} async-done(((f32[256,2048]{1,0:T(8,128)}), f32[16,2048]{1,0:T(8,128)}) %reduce-scatter.4.cloned.1.call-update) | async-done | bytes 131088 | tf_op jit(solution)/shard_map/reduce_scatter | solution.py:55
  219.9 0.0 copy-done.4
  219.9 0.0 copy-done.5
  219.9 0.0 copy-done.7
  219.9 1.6 add_divide_fusion
  221.5 0.0 all-gather.13.cloned.1.call-update
  221.5 0.0 all-gather.11.cloned.1.call-start
  221.6 0.5 all-gather.11.cloned.1.call-update
  222.1 0.0 all-gather.15.cloned.1.call-start
  222.2 2.0 copy.59
  224.2 50.4 %all-gather.13.cloned.1.call-done = f32[256,1024]{1,0:T(8,128)} async-done(((f32[16,1024]{1,0:T(8,128)}), f32[256,1024]{1,0:T(8,128)}) %all-gather.13.cloned.1.call-update) | async-done | bytes 1048592 | tf_op jit(solution)/shard_map/all_gather | solution.py:63
  274.6 0.0 copy-done.2
  274.6 3.7 multiply_reduce_fusion
  278.3 53.4 %all-gather.11.cloned.1.call-done = f32[256,1024]{1,0:T(8,128)} async-done(((f32[16,1024]{1,0:T(8,128)}), f32[256,1024]{1,0:T(8,128)}) %all-gather.11.cloned.1.call-update) | async-done | bytes 1048592 | tf_op jit(solution)/shard_map/all_gather | solution.py:62
  331.7 3.6 multiply_reduce_fusion.1
  335.4 38.6 %all-reduce = (f32[]{:T(128)}, f32[]{:T(128)}) all-reduce(f32[]{:T(128)} %get-tuple-element.47, f32[]{:T(128)} %get-tuple-element.49), channel_id=1, replica_groups=mesh['fs'=16,'tp'=2] {'fs','tp'}, use_global_device_ids=true, to_apply=%region_2.0 | all-reduce | flops 2 | bytes 16 | tf_op jit(solution)/shard_map/psum | solution.py:68
  374.7 2.2 subtract_convert_fusion.1
  376.8 0.0 all-gather.15.cloned.1.call-update
  376.9 0.0 all-gather.17.cloned.1.call-start
  376.9 2.0 copy.60
  379.7 2.2 subtract_convert_fusion
  381.8 0.0 all-gather.17.cloned.1.call-update
  381.9 2.0 copy.61
  383.9 2.0 copy.62
  385.9 80.5 %all-gather.15.cloned.1.call-done = bf16[2048,1024]{0,1:T(8,128)(2,1)} async-done(((bf16[128,1024]{0,1:T(8,128)(2,1)}), bf16[2048,1024]{0,1:T(8,128)(2,1)}) %all-gather.15.cloned.1.call-update) | async-done | bytes 4194320 | tf_op jit(solution)/shard_map/all_gather | solution.py:76
  466.4 6.4 %copy.63 = bf16[2048,1024]{1,0:T(8,128)(2,1)} copy(bf16[2048,1024]{0,1:T(8,128)(2,1)} %all-gather.15.cloned.1.call-done) | data formatting | bytes 8388608
  472.8 83.2 %all-gather.17.cloned.1.call-done = bf16[2048,1024]{0,1:T(8,128)(2,1)} async-done(((bf16[128,1024]{0,1:T(8,128)(2,1)}), bf16[2048,1024]{0,1:T(8,128)(2,1)}) %all-gather.17.cloned.1.call-update) | async-done | bytes 4194320 | tf_op jit(solution)/shard_map/all_gather | solution.py:77
  556.0 6.4 %copy.64 = bf16[2048,1024]{1,0:T(8,128)(2,1)} copy(bf16[2048,1024]{0,1:T(8,128)(2,1)} %all-gather.17.cloned.1.call-done) | data formatting | bytes 8388608
  (9 shorter events, 0.0 us)
Async XLA Ops:
  7.2 1.9 copy-start
  7.2 61.4 %all-gather.7.cloned.1.call-start = ((), (), s32[]{:S(2)}) async-start(), calls=%async_computation.1 | async-start | bytes 1114112 | tf_op jit(solution)/shard_map/all_gather | solution.py:42
  7.9 117.4 %all-gather.9.cloned.1.call-start = ((), (), s32[]{:S(2)}) async-start(), calls=%async_computation.2 | async-start | bytes 1114112 | tf_op jit(solution)/shard_map/all_gather | solution.py:43
  8.7 211.2 %reduce-scatter.4.cloned.1.call-start = ((), (), s32[]{:S(2)}) async-start(), calls=%async_computation.7 | async-start | bytes 2228224 | tf_op jit(solution)/shard_map/reduce_scatter | solution.py:55
  9.1 7.2 %copy-start.8 = (bf16[768,1024]{1,0:T(8,128)(2,1)S(1)}, bf16[768,1024]{1,0:T(8,128)(2,1)}, u32[]{:S(2)}) copy-start(bf16[768,1024]{1,0:T(8,128)(2,1)} %param.13) | copy-start | bytes 4718596
  125.3 9.5 %copy-start.1 = (f32[256,1024]{0,1:T(8,128)S(1)}, f32[256,1024]{0,1:T(8,128)}, u32[]{:S(2)}) copy-start(f32[256,1024]{0,1:T(8,128)} %convolution_bitcast_fusion.1) | copy-start | bytes 3145732
  136.2 83.6 %copy-start.4 = (f32[16,1024]{1,0:T(8,128)S(1)}, f32[16,1024]{1,0:T(8,128)}, u32[]{:S(2)}) copy-start(f32[16,1024]{1,0:T(8,128)} %param.21) | copy-start | bytes 196612
  136.2 83.6 %copy-start.5 = (f32[16,1024]{1,0:T(8,128)S(1)}, f32[16,1024]{1,0:T(8,128)}, u32[]{:S(2)}) copy-start(f32[16,1024]{1,0:T(8,128)} %param.20) | copy-start | bytes 196612
  136.2 83.6 %copy-start.6 = (f32[16,1024]{1,0:T(8,128)S(1)}, f32[16,1024]{1,0:T(8,128)}, u32[]{:S(2)}) copy-start(f32[16,1024]{1,0:T(8,128)} %param.19) | copy-start | bytes 196612
  136.2 83.6 %copy-start.7 = (f32[16,1024]{1,0:T(8,128)S(1)}, f32[16,1024]{1,0:T(8,128)}, u32[]{:S(2)}) copy-start(f32[16,1024]{1,0:T(8,128)} %param.18) | copy-start | bytes 196612
  136.2 138.3 %copy-start.2 = (bf16[128,256]{1,0:T(8,128)(2,1)S(1)}, bf16[128,256]{1,0:T(8,128)(2,1)}, u32[]{:S(2)}) copy-start(bf16[128,256]{1,0:T(8,128)(2,1)} %param.17) | copy-start | bytes 196612
  139.2 192.5 %copy-start.3 = (bf16[128,256]{1,0:T(8,128)(2,1)S(1)}, bf16[128,256]{1,0:T(8,128)(2,1)}, u32[]{:S(2)}) copy-start(bf16[128,256]{1,0:T(8,128)(2,1)} %param.16) | copy-start | bytes 196612
  139.2 135.4 %all-gather.13.cloned.1.call-start = ((), (), s32[]{:S(2)}) async-start(), calls=%async_computation.4 | async-start | bytes 1114112 | tf_op jit(solution)/shard_map/all_gather | solution.py:63
  221.5 110.2 %all-gather.11.cloned.1.call-start = ((), (), s32[]{:S(2)}) async-start(), calls=%async_computation.3 | async-start | bytes 1114112 | tf_op jit(solution)/shard_map/all_gather | solution.py:62
  222.1 244.3 %all-gather.15.cloned.1.call-start = ((), (), s32[]{:S(2)}) async-start(), calls=%async_computation.5 | async-start | bytes 4456448 | tf_op jit(solution)/shard_map/all_gather | solution.py:76
  376.9 179.2 %all-gather.17.cloned.1.call-start = ((), (), s32[]{:S(2)}) async-start(), calls=%async_computation.6 | async-start | bytes 4456448 | tf_op jit(solution)/shard_map/all_gather | solution.py:77
Sparse Core Ops, SparseCore 0:
  10.7 57.7 all-gather.6
  71.3 53.9 all-gather.8
  139.3 80.4 reduce-scatter.3
  223.0 51.4 all-gather.12
  277.8 53.9 all-gather.10
  377.0 89.3 all-gather.14
  469.1 86.8 all-gather.16
where the time goes:
time: 570 us; the launch traced here: 569 us
  waiting for transfers between devices  442 us (78%)
  matrix products  40.9 us (7%)
  blocking collectives  38.6 us (7%)
  local copies, waits for them, and re-layouts  24.3 us (4%)
  between operations  15.6 us (3%)
  other arithmetic  7.42 us (1%)
    all_gather x1, waiting for transfers between devices, local(): lax.all_gather(local_gate, 'fs', axis=0, tiled=True)  83.2 us
    reduce_scatter x1, waiting for transfers between devices, local(): lax.psum_scatter(jnp.concatenate([term_in, term_gate], axis=1), 'fs', sca...  80.6 us
    all_gather x1, waiting for transfers between devices, local(): lax.all_gather(local_in, 'fs', axis=0, tiled=True)  80.5 us
    all_gather x1, waiting for transfers between devices, local(): piece_in = lax.all_gather(ratio_in, 'fs', axis=0, tiled=True)  53.4 us
    all_gather x1, waiting for transfers between devices, local(): piece_gate = lax.all_gather(ratio_gate, 'fs', axis=0, tiled=True)  50.4 us
    all_gather x1, waiting for transfers between devices, local(): lax.all_gather(input_factor, 'fs', axis=0, tiled=True)  46.7 us
    all_gather x1, waiting for transfers between devices, local(): lax.all_gather(gate_factor, 'fs', axis=0, tiled=True)  45.5 us
    psum x1, blocking collectives, local(): lax.psum((jnp.sum(dir_in * dir_in), jnp.sum(dir_gate * dir_gate)), ('fs',...  38.6 us
  transfers between devices with their start and end apart: 7, of which 7 were waited for; matrix products, arithmetic and copies ran while one was open for 8% of the time, Pallas kernels for 0%

commit v1 on v0

v1 whole, which is shorter than its diff:
```python
import functools

import jax
import jax.numpy as jnp
from jax import lax
from jax.experimental import pallas as pl
from jax.experimental.pallas import tpu as pltpu
from jax.sharding import PartitionSpec as P

first_decay = 0.9
second_decay = 0.9
ratio_floor = 1e-08
mean_floor = 1e-06
step_size = 0.05
PLANE = 4
VMEM = pltpu.VMEM
DMA = pltpu.SemaphoreType.DMA
MESH = pl.DeviceIdType.MESH


class Place:
    def __init__(self, n):
        self.n = n
        self.depth = n // PLANE
        self.f = lax.axis_index("fs")
        self.z = lax.div(self.f, PLANE)
        self.spot = lax.rem(self.f, PLANE)
        self.x = lax.rem(self.f, 2)
        self.y = lax.div(self.spot, 2)
        self.fx = self.f + 1 - 2 * self.x
        self.fy = self.f + 2 - 4 * self.y
        self.sx = self.spot + 1 - 2 * self.x
        self.sy = self.spot + 2 - 4 * self.y

    def plane(self, dz):
        return lax.rem(self.z + dz + self.depth, self.depth)


def send(src, dst, s_sem, r_sem, axis, target):
    return pltpu.make_async_remote_copy(
        src_ref=src,
        dst_ref=dst,
        send_sem=s_sem,
        recv_sem=r_sem,
        device_id={axis: target},
        device_id_type=MESH,
    )


def greet(targets):
    barrier = pltpu.get_barrier_semaphore()
    for axis, target in targets:
        pl.semaphore_signal(barrier, inc=1, device_id={axis: target}, device_id_type=MESH)
    pl.semaphore_wait(barrier, len(targets))


def gather(at, a, b, s_z, r_z, s_p, r_p):
    depth = at.depth
    started = []

    def go(copy):
        copy.start()
        started.append(copy)
        return copy

    far = [None]
    for dz in range(1, depth):
        target = at.plane(dz) * PLANE + at.spot
        far.append(
            (
                go(send(a.at[at.f], a.at[at.f], s_z.at[dz, 0], r_z.at[dz, 0], "fs", target)),
                go(send(b.at[at.f], b.at[at.f], s_z.at[dz, 1], r_z.at[dz, 1], "fs", target)),
            )
        )
    near = []
    for s in range(depth + 1):
        if s < depth:
            base = at.plane(-s) * PLANE
            mine = base + at.spot

            def own(ref, k, target):
                return go(send(ref.at[mine], ref.at[mine], s_p.at[s, k], r_p.at[s, k], "fs", target))

            if s > 0:
                far[s][0].wait_recv()
            xa = own(a, 0, at.fx)
            ya = own(a, 1, at.fy)
            if s > 0:
                far[s][1].wait_recv()
            yb = own(b, 2, at.fy)
            xb = own(b, 3, at.fx)
            near.append((base, xa, ya, yb, xb))
        if s > 0:
            base, xa, ya, yb, xb = near[s - 1]
            xa.wait_recv()
            got = base + at.sx
            ra = go(send(a.at[got], a.at[got], s_p.at[s - 1, 4], r_p.at[s - 1, 4], "fs", at.fy))
            yb.wait_recv()
            got = base + at.sy
            rb = go(send(b.at[got], b.at[got], s_p.at[s - 1, 5], r_p.at[s - 1, 5], "fs", at.fx))
            near[s - 1] = (ya, xb, ra, rb)
    for group in near:
        for copy in group:
            copy.wait_recv()
    for copy in started:
        copy.wait_send()


def near_targets(at):
    return [("fs", at.fx), ("fs", at.fy)] + [
        ("fs", at.plane(dz) * PLANE + at.spot) for dz in range(1, at.depth)
    ]


def factor_kernel(n, a_ref, b_ref, a_out, b_out, s_z, r_z, s_p, r_p):
    at = Place(n)
    a_out[at.f] = a_ref[...]
    b_out[at.f] = b_ref[...]
    greet(near_targets(at))
    gather(at, a_out, b_out, s_z, r_z, s_p, r_p)


def gather_sems(n):
    depth = n // PLANE
    return [DMA((depth, 2)), DMA((depth, 2)), DMA((depth, 6)), DMA((depth, 6))]


def moments(low_rank, first, second):
    first_new = first_decay * first + (1.0 - first_decay) * low_rank
    second_new = second_decay * second + (1.0 - second_decay) * low_rank * low_rank
    ratio = first_new / (jnp.sqrt(second_new) + ratio_floor)
    return (first_new, second_new, ratio)


def wide_dot(narrow, wide):
    total = None
    rest = wide
    for _ in range(3):
        part = rest.astype(jnp.bfloat16)
        rest = rest - part.astype(jnp.float32)
        term = jnp.dot(narrow, part, preferred_element_type=jnp.float32)
        total = term if total is None else total + term
    return total


def main_kernel(
    n,
    m,
    term_a,
    term_b,
    first_a,
    second_a,
    first_b,
    second_b,
    factor_a,
    factor_b,
    master_a,
    master_b,
    step_a,
    step_b,
    first_a_new,
    second_a_new,
    first_b_new,
    second_b_new,
    copy_a,
    copy_b,
    one_a,
    one_b,
    two_a,
    two_b,
    sum_a,
    sum_b,
    ready_a,
    ready_b,
    far_a,
    far_b,
    all_a,
    all_b,
    pair,
    total,
    s_one,
    r_one,
    s_two,
    r_two,
    s_far,
    r_far,
    rz_s,
    rz_r,
    rp_s,
    rp_r,
    s_tp,
    r_tp,
    s_fs,
    r_fs,
    cz_s,
    cz_r,
    cp_s,
    cp_r,
):
    at = Place(n)
    depth = at.depth
    t = lax.axis_index("tp")
    others = [lax.rem(at.f + k, n) for k in range(1, n)]
    mates = [lax.rem(t + k, m) for k in range(1, m)]
    greet([("fs", o) for o in others] + [("tp", o) for o in mates])
    started = []

    def go(copy):
        copy.start()
        started.append(copy)
        return copy

    first_stage = []
    for k in range(depth):
        plane = at.plane(k + 1)
        pair_a = go(send(term_a.at[plane, :, 1 - at.x], one_a.at[k], s_one.at[k, 0], r_one.at[k, 0], "fs", at.fx))
        pair_b = go(send(term_b.at[plane, 1 - at.y], one_b.at[k], s_one.at[k, 1], r_one.at[k, 1], "fs", at.fy))
        first_stage.append((pair_a, pair_b))
    second_stage = []
    third_stage = []
    for k in range(depth + 1):
        if k < depth:
            plane = at.plane(k + 1)
            first_stage[k][0].wait_recv()
            sum_a[k] = term_a[plane, :, at.x] + one_a[k]
            ca = go(send(sum_a.at[k, 1 - at.y], two_a.at[k], s_two.at[k, 0], r_two.at[k, 0], "fs", at.fy))
            first_stage[k][1].wait_recv()
            sum_b[k] = term_b[plane, at.y] + one_b[k]
            cb = go(send(sum_b.at[k, 1 - at.x], two_b.at[k], s_two.at[k, 1], r_two.at[k, 1], "fs", at.fx))
            second_stage.append((ca, cb))
        if k > 0:
            j = k - 1
            target = at.plane(k) * PLANE + at.spot
            second_stage[j][0].wait_recv()
            ready_a[j] = sum_a[j, at.y] + two_a[j]
            if j < depth - 1:
                ca = go(send(ready_a.at[j], far_a.at[j], s_far.at[j, 0], r_far.at[j, 0], "fs", target))
            second_stage[j][1].wait_recv()
            ready_b[j] = sum_b[j, at.x] + two_b[j]
            if j < depth - 1:
                cb = go(send(ready_b.at[j], far_b.at[j], s_far.at[j, 1], r_far.at[j, 1], "fs", target))
                third_stage.append((ca, cb))
    low_a = ready_a[depth - 1]
    low_b = ready_b[depth - 1]
    for j in range(depth - 1):
        third_stage[j][0].wait_recv()
        low_a = low_a + far_a[j]
        third_stage[j][1].wait_recv()
        low_b = low_b + far_b[j]

    new_first, new_second, ratio = moments(low_a, first_a[...], second_a[...])
    first_a_new[...] = new_first
    second_a_new[...] = new_second
    all_a[at.f] = ratio
    new_first, new_second, ratio = moments(low_b, first_b[...], second_b[...])
    first_b_new[...] = new_first
    second_b_new[...] = new_second
    all_b[at.f] = ratio

    gather(at, all_a, all_b, rz_s, rz_r, rp_s, rp_r)

    rank = all_a.shape[0] * all_a.shape[1]
    cols = all_a.shape[2]
    dir_a = wide_dot(factor_a[...], all_a[...].reshape(rank, cols))
    dir_b = wide_dot(factor_b[...], all_b[...].reshape(rank, cols))
    count = n * dir_a.shape[0] * m * cols

    pair[0, 0:8] = jnp.full((8, 128), jnp.sum(dir_a * dir_a), jnp.float32)
    pair[0, 8:16] = jnp.full((8, 128), jnp.sum(dir_b * dir_b), jnp.float32)
    trips = [
        go(send(pair.at[0], pair.at[k + 1], s_tp.at[k], r_tp.at[k], "tp", mate)) for k, mate in enumerate(mates)
    ]
    step_a[...] = dir_a
    step_b[...] = dir_b
    joint = pair[0]
    for k, trip in enumerate(trips):
        trip.wait_recv()
        joint = joint + pair[k + 1]
    total[0] = joint
    trips = [
        go(send(total.at[0], total.at[k + 1], s_fs.at[k], r_fs.at[k], "fs", other)) for k, other in enumerate(others)
    ]
    joint = total[0]
    for k, trip in enumerate(trips):
        trip.wait_recv()
        joint = joint + total[k + 1]
    scale = lax.rsqrt(joint / count + mean_floor)
    new_step = step_a[...] * scale[0:1, 0:1]
    step_a[...] = new_step
    copy_a[at.f] = (master_a[...] - step_size * new_step).astype(jnp.bfloat16)
    new_step = step_b[...] * scale[8:9, 0:1]
    step_b[...] = new_step
    copy_b[at.f] = (master_b[...] - step_size * new_step).astype(jnp.bfloat16)

    gather(at, copy_a, copy_b, cz_s, cz_r, cp_s, cp_r)
    for copy in started:
        copy.wait_send()


def local(
    n,
    m,
    saved_inputs,
    input_cot,
    gate_cot,
    input_master,
    gate_master,
    input_factor,
    gate_factor,
    input_first,
    input_second,
    gate_first,
    gate_second,
):
    in_vmem = pl.BlockSpec(memory_space=VMEM)
    rows, rank = input_factor.shape
    low_rows, cols = input_first.shape
    depth = n // PLANE
    shape = jax.ShapeDtypeStruct
    f32, bf16 = jnp.float32, jnp.bfloat16
    whole_in, whole_gate = pl.pallas_call(
        functools.partial(factor_kernel, n),
        out_shape=[shape((n, rows, rank), bf16)] * 2,
        in_specs=[in_vmem] * 2,
        out_specs=[in_vmem] * 2,
        scratch_shapes=gather_sems(n),
        compiler_params=pltpu.CompilerParams(collective_id=0, has_side_effects=True),
        name="factors",
    )(input_factor, gate_factor)

    def term(whole, cot):
        mid = jnp.dot(saved_inputs, whole.reshape(n * rows, rank), preferred_element_type=f32)
        low = lax.dot_general(
            mid, cot.astype(f32), (((0,), (0,)), ((), ())), precision=lax.Precision.HIGHEST
        )
        return low.reshape(depth, 2, 2, low_rows, cols)

    term_in = term(whole_in, input_cot)
    term_gate = term(whole_gate, gate_cot)
    low = shape((low_rows, cols), f32)
    piece = (low_rows, cols)
    full = shape((rows, cols), f32)
    copies = shape((n, rows, cols), bf16)
    outs = pl.pallas_call(
        functools.partial(main_kernel, n, m),
        out_shape=[full, full, low, low, low, low, copies, copies],
        in_specs=[in_vmem] * 10,
        out_specs=[in_vmem] * 8,
        scratch_shapes=[
            VMEM((depth, 2) + piece, f32),
            VMEM((depth, 2) + piece, f32),
            VMEM((depth,) + piece, f32),
            VMEM((depth,) + piece, f32),
            VMEM((depth, 2) + piece, f32),
            VMEM((depth, 2) + piece, f32),
            VMEM((depth,) + piece, f32),
            VMEM((depth,) + piece, f32),
            VMEM((depth,) + piece, f32),
            VMEM((depth,) + piece, f32),
            VMEM((n,) + piece, f32),
            VMEM((n,) + piece, f32),
            VMEM((m, 16, 128), f32),
            VMEM((n, 16, 128), f32),
            DMA((depth, 2)),
            DMA((depth, 2)),
            DMA((depth, 2)),
            DMA((depth, 2)),
            DMA((depth, 2)),
            DMA((depth, 2)),
            *gather_sems(n),
            DMA((m,)),
            DMA((m,)),
            DMA((n,)),
            DMA((n,)),
            *gather_sems(n),
        ],
        compiler_params=pltpu.CompilerParams(
            collective_id=1, has_side_effects=True, vmem_limit_bytes=56 * 2**20
        ),
        name="update",
    )(
        term_in,
        term_gate,
        input_first,
        input_second,
        gate_first,
        gate_second,
        input_factor,
        gate_factor,
        input_master,
        gate_master,
    )
    *head, copy_in, copy_gate = outs
    return (*head, copy_in.reshape(n * rows, cols), copy_gate.reshape(n * rows, cols))


def solution(mesh):
    n, m = mesh.shape["fs"], mesh.shape["tp"]
    both = P("fs", "tp")
    rows = P("fs", None)
    return jax.shard_map(
        functools.partial(local, n, m),
        mesh=mesh,
        in_specs=(rows, both, both, both, both, rows, rows, both, both, both, both),
        out_specs=(both,) * 6 + (P(None, "tp"),) * 2,
        check_vma=False,
    )
```

time: 570 us -> 201 us (0.35)
  the two profiles are of different devices: /device:TPU:0 before, /device:TPU:24 now
where the time goes in v1:
time: 201 us
  Pallas kernels  175 us (87%)
  local copies, waits for them, and re-layouts  16.8 us (8%)
  matrix products  8.19 us (4%)
    pallas_call x1, Pallas kernels, local(): pl.pallas_call(functools.partial(main_kernel, n, m), out_shape=[full, ful...  144 us
    pallas_call x1, Pallas kernels, local(): pl.pallas_call(functools.partial(factor_kernel, n), out_shape=[shape((n,...  30.4 us
    unnamed x18, local copies, waits for them, and re-layouts  16.8 us
    dot_general x2, matrix products, term(): lax.dot_general(mid, cot.astype(f32), (((0,), (0,)), ((), ())), precision...  4.78 us

profile of v1, /device:TPU:24, one launch (start us, length us, event | category | flops | bytes accessed | tf_op | source)
XLA Modules:
  0.0 200.6 jit_solution(5762998793234568809)
XLA Ops:
  0.6 0.0 copy-start
  0.6 30.4 %factors.1 = (bf16[16,128,256]{2,1,0:T(8,128)(2,1)}, bf16[16,128,256]{2,1,0:T(8,128)(2,1)}) custom-call(bf16[128,256]{1,0:T(8,128)(2,1)} %factor_a.1, bf16[128,256]{1,0:T(8,128)(2,1)} %factor_b.1), custom_call_target="tpu_custom_call" | custom-call | tf_op jit(solution)/shard_map/factors/pallas_call | solution.py:321
  31.0 0.0 copy-start.4
  31.1 0.0 copy-done
  31.1 2.3 %fusion = f32[256,768]{1,0:T(8,128)S(1)} fusion(bf16[2048,256]{1,0:T(8,128)(2,1)} %bitcast.19, bf16[768,2048]{1,0:T(8,128)(2,1)S(1)} %copy-done), kind=kOutput, calls=%fused_computation | convolution fusion | flops 805306368 | bytes 4980736 | tf_op jit(solution)/shard_map/dot_general | solution.py:332
  33.4 0.0 copy-start.2
  33.4 0.0 copy-done.4
  33.4 0.0 copy-start.3
  33.4 1.1 fusion.2
  34.5 0.3 copy-done.2
  34.8 2.4 %fusion.3 = f32[256,1024]{1,0:T(8,128)} fusion(f32[256,768]{1,0:T(8,128)S(1)} %fusion.2, bf16[768,1024]{1,0:T(8,128)(2,1)S(1)} %copy-done.2), kind=kOutput, calls=%fused_computation.3 | convolution fusion | flops 2415919104 | bytes 3407872 | tf_op jit(solution)/shard_map/dot_general | solution.py:333
  37.2 0.0 copy-done.3
  37.2 2.4 %fusion.1 = f32[256,1024]{1,0:T(8,128)} fusion(f32[256,768]{1,0:T(8,128)S(1)} %fusion, bf16[768,1024]{1,0:T(8,128)(2,1)S(1)} %copy-done.3), kind=kOutput, calls=%fused_computation.1 | convolution fusion | flops 2415919104 | bytes 3407872 | tf_op jit(solution)/shard_map/dot_general | solution.py:333
  39.6 144.5 %update.1 = (f32[128,1024]{1,0:T(8,128)}, f32[128,1024]{1,0:T(8,128)}, f32[16,1024]{1,0:T(8,128)}, f32[16,1024]{1,0:T(8,128)}, f32[16,1024]{1,0:T(8,128)}, /*ind...) custom-call(f32[4,2,2,16,1024]{4,3,2,1,0:T(8,128)} %bitcast.15, ...), custom_call_target="tpu_custom_call" | custom-call | tf_op jit(solution)/shard_map/update/pallas_call | solution.py:344
  184.1 1.9 copy.27
  186.0 1.9 copy.28
  187.9 1.5 copy.29
  189.3 1.5 copy.30
  190.8 1.5 copy.31
  192.3 1.5 copy.32
  193.7 0.0 copy-start.1
  193.7 4.8 %copy.33 = bf16[2048,1024]{1,0:T(8,128)(2,1)} copy(bf16[2048,1024]{1,0:T(8,128)(2,1)} %bitcast.17) | data formatting | bytes 8388608
  198.6 0.0 copy-done.1
  198.6 2.0 %copy.34 = bf16[2048,1024]{1,0:T(8,128)(2,1)} copy(bf16[2048,1024]{1,0:T(8,128)(2,1)S(1)} %bitcast.16) | data formatting | bytes 8388608
Async XLA Ops:
  0.6 30.4 %copy-start = (bf16[768,2048]{1,0:T(8,128)(2,1)S(1)}, bf16[768,2048]{1,0:T(8,128)(2,1)}, u32[]{:S(2)}) copy-start(bf16[768,2048]{1,0:T(8,128)(2,1)} %param.11) | copy-start | bytes 9437188
  31.0 2.4 %copy-start.4 = (bf16[16,128,256]{2,1,0:T(8,128)(2,1)S(1)}, bf16[16,128,256]{2,1,0:T(8,128)(2,1)}, u32[]{:S(2)}) copy-start(bf16[16,128,256]{2,1,0:T(8,128)(2,1)} %get-tuple-element.19) | copy-start | bytes 3145732
  33.4 1.4 copy-start.2
  33.4 3.8 %copy-start.3 = (bf16[768,1024]{1,0:T(8,128)(2,1)S(1)}, bf16[768,1024]{1,0:T(8,128)(2,1)}, u32[]{:S(2)}) copy-start(bf16[768,1024]{1,0:T(8,128)(2,1)} %param.12) | copy-start | bytes 4718596
  193.7 4.8 %copy-start.1 = (bf16[16,128,1024]{2,1,0:T(8,128)(2,1)S(1)}, bf16[16,128,1024]{2,1,0:T(8,128)(2,1)}, u32[]{:S(2)}) copy-start(bf16[16,128,1024]{2,1,0:T(8,128)(2,1)} %get-tuple-element.27) | copy-start | bytes 12582916

commit v2 on v1

--- a/solution.py
+++ b/solution.py
@@ -32,8 +32,14 @@
         self.sx = self.spot + 1 - 2 * self.x
         self.sy = self.spot + 2 - 4 * self.y
 
-    def plane(self, dz):
-        return lax.rem(self.z + dz + self.depth, self.depth)
+    def twin(self, s):
+        other = self.z
+        bit = 1
+        while bit <= s:
+            if s // bit % 2:
+                other = other + bit - 2 * bit * lax.rem(lax.div(self.z, bit), 2)
+            bit *= 2
+        return other
 
 
 def send(src, dst, s_sem, r_sem, axis, target):
@@ -54,70 +60,58 @@
     pl.semaphore_wait(barrier, len(targets))
 
 
-def gather(at, a, b, s_z, r_z, s_p, r_p):
+def whole_block(ref, index):
+    return ref.at[index]
+
+
+def gather(at, a, b, s_z, r_z, s_p, r_p, view=whole_block, arrived=None):
     depth = at.depth
     started = []
 
-    def go(copy):
+    def go(ref, index, s_sem, r_sem, target):
+        copy = send(view(ref, index), view(ref, index), s_sem, r_sem, "fs", target)
         copy.start()
         started.append(copy)
         return copy
 
     far = [None]
-    for dz in range(1, depth):
-        target = at.plane(dz) * PLANE + at.spot
+
+    def reach(dz):
+        target = at.twin(dz) * PLANE + at.spot
         far.append(
             (
-                go(send(a.at[at.f], a.at[at.f], s_z.at[dz, 0], r_z.at[dz, 0], "fs", target)),
-                go(send(b.at[at.f], b.at[at.f], s_z.at[dz, 1], r_z.at[dz, 1], "fs", target)),
+                go(a, at.f, s_z.at[dz, 0], r_z.at[dz, 0], target),
+                go(b, at.f, s_z.at[dz, 1], r_z.at[dz, 1], target),
             )
         )
+
     near = []
-    for s in range(depth + 1):
-        if s < depth:
-            base = at.plane(-s) * PLANE
-            mine = base + at.spot
-
-            def own(ref, k, target):
-                return go(send(ref.at[mine], ref.at[mine], s_p.at[s, k], r_p.at[s, k], "fs", target))
-
-            if s > 0:
-                far[s][0].wait_recv()
-            xa = own(a, 0, at.fx)
-            ya = own(a, 1, at.fy)
-            if s > 0:
-                far[s][1].wait_recv()
-            yb = own(b, 2, at.fy)
-            xb = own(b, 3, at.fx)
-            near.append((base, xa, ya, yb, xb))
+    for s in range(depth):
+        base = at.twin(s) * PLANE
+        mine = base + at.spot
         if s > 0:
-            base, xa, ya, yb, xb = near[s - 1]
-            xa.wait_recv()
-            got = base + at.sx
-            ra = go(send(a.at[got], a.at[got], s_p.at[s - 1, 4], r_p.at[s - 1, 4], "fs", at.fy))
-            yb.wait_recv()
-            got = base + at.sy
-            rb = go(send(b.at[got], b.at[got], s_p.at[s - 1, 5], r_p.at[s - 1, 5], "fs", at.fx))
-            near[s - 1] = (ya, xb, ra, rb)
-    for group in near:
+            far[s][0].wait_recv()
+        xa = go(a, mine, s_p.at[s, 0], r_p.at[s, 0], at.fx)
+        ya = go(a, mine, s_p.at[s, 1], r_p.at[s, 1], at.fy)
+        if s > 0:
+            far[s][1].wait_recv()
+        yb = go(b, mine, s_p.at[s, 2], r_p.at[s, 2], at.fy)
+        xb = go(b, mine, s_p.at[s, 3], r_p.at[s, 3], at.fx)
+        if s == 0:
+            for dz in range(1, depth):
+                reach(dz)
+        xa.wait_recv()
+        ra = go(a, base + at.sx, s_p.at[s, 4], r_p.at[s, 4], at.fy)
+        yb.wait_recv()
+        rb = go(b, base + at.sy, s_p.at[s, 5], r_p.at[s, 5], at.fx)
+        near.append((base, ya, xb, ra, rb))
+    for base, *group in near:
         for copy in group:
             copy.wait_recv()
+        if arrived is not None:
+            arrived(base)
     for copy in started:
         copy.wait_send()
-
-
-def near_targets(at):
-    return [("fs", at.fx), ("fs", at.fy)] + [
-        ("fs", at.plane(dz) * PLANE + at.spot) for dz in range(1, at.depth)
-    ]
-
-
-def factor_kernel(n, a_ref, b_ref, a_out, b_out, s_z, r_z, s_p, r_p):
-    at = Place(n)
-    a_out[at.f] = a_ref[...]
-    b_out[at.f] = b_ref[...]
-    greet(near_targets(at))
-    gather(at, a_out, b_out, s_z, r_z, s_p, r_p)
 
 
 def gather_sems(n):
@@ -146,22 +140,36 @@
 def main_kernel(
     n,
     m,
-    term_a,
-    term_b,
+    saved_hbm,
+    cot_a_hbm,
+    cot_b_hbm,
+    master_a_hbm,
+    master_b_hbm,
+    factor_a,
+    factor_b,
     first_a,
     second_a,
     first_b,
     second_b,
-    factor_a,
-    factor_b,
-    master_a,
-    master_b,
     step_a,
     step_b,
     first_a_new,
     second_a_new,
     first_b_new,
     second_b_new,
+    copy_a_hbm,
+    copy_b_hbm,
+    saved,
+    cot_a,
+    cot_b,
+    master_a,
+    master_b,
+    whole_a,
+    whole_b,
+    mid_a,
+    mid_b,
+    term_a,
+    term_b,
     copy_a,
     copy_b,
     one_a,
@@ -178,12 +186,20 @@
     all_b,
     pair,
     total,
+    load_sem,
+    store_sem,
+    s_mate,
+    r_mate,
     s_one,
     r_one,
     s_two,
     r_two,
     s_far,
     r_far,
+    fz_s,
+    fz_r,
+    fp_s,
+    fp_r,
     rz_s,
     rz_r,
     rp_s,
@@ -202,6 +218,22 @@
     t = lax.axis_index("tp")
     others = [lax.rem(at.f + k, n) for k in range(1, n)]
     mates = [lax.rem(t + k, m) for k in range(1, m)]
+    loads = [
+        pltpu.make_async_copy(src, dst, load_sem.at[k])
+        for k, (src, dst) in enumerate(
+            (
+                (saved_hbm, saved),
+                (cot_a_hbm, cot_a),
+                (cot_b_hbm, cot_b),
+                (master_a_hbm, master_a),
+                (master_b_hbm, master_b),
+            )
+        )
+    ]
+    for load in loads:
+        load.start()
+    whole_a[at.f] = factor_a[...]
+    whole_b[at.f] = factor_b[...]
     greet([("fs", o) for o in others] + [("tp", o) for o in mates])
     started = []
 
@@ -210,17 +242,72 @@
         started.append(copy)
         return copy
 
+    rows = factor_a.shape[0]
+    parts = 2 if m % 2 == 0 else 1
+    mate = t + 1 - 2 * lax.rem(t, 2)
+    half = pl.ds(pl.multiple_of(lax.rem(t, 2) * (rows // 2), rows // 2), rows // 2) if parts == 2 else pl.ds(0, rows)
+    passed = []
+    width = PLANE * rows
+
+    def multiply(k):
+        base, copies = passed[k]
+        for copy in copies:
+            copy.wait_recv()
+        if k == 0:
+            loads[0].wait()
+        columns = pl.ds(pl.multiple_of(base * rows, width), width)
+        for mid, whole in ((mid_a, whole_a), (mid_b, whole_b)):
+            block = whole[pl.ds(base, PLANE)].reshape(width, whole.shape[2])
+            product = jnp.dot(saved[:, columns], block, preferred_element_type=jnp.float32)
+            if k == 0:
+                mid[...] = product
+            else:
+                mid[...] += product
+
+    def arrived(base):
+        k = len(passed)
+        copies = []
+        if parts == 2:
+            for side, whole in enumerate((whole_a, whole_b)):
+                view = whole.at[pl.ds(base, PLANE), half]
+                copies.append(go(send(view, view, s_mate.at[k, side], r_mate.at[k, side], "tp", mate)))
+        passed.append((base, copies))
+        if k > 0:
+            multiply(k - 1)
+
+    gather(at, whole_a, whole_b, fz_s, fz_r, fp_s, fp_r, lambda ref, index: ref.at[index, half], arrived)
+    multiply(depth - 1)
+
+    def project(mid, cot):
+        rest = mid[...].T
+        result = None
+        for _ in range(3):
+            part = rest.astype(jnp.bfloat16)
+            rest = rest - part.astype(jnp.float32)
+            piece = jnp.dot(part, cot[...], preferred_element_type=jnp.float32)
+            result = piece if result is None else result + piece
+        return result
+
+    loads[1].wait()
+    term_a[...] = project(mid_a, cot_a).reshape(term_a.shape)
+    first_a_stage = []
+    for k in range(depth):
+        plane = at.twin(depth - 1 - k)
+        first_a_stage.append(
+            go(send(term_a.at[plane, :, 1 - at.x], one_a.at[k], s_one.at[k, 0], r_one.at[k, 0], "fs", at.fx))
+        )
+    loads[2].wait()
+    term_b[...] = project(mid_b, cot_b).reshape(term_b.shape)
     first_stage = []
     for k in range(depth):
-        plane = at.plane(k + 1)
-        pair_a = go(send(term_a.at[plane, :, 1 - at.x], one_a.at[k], s_one.at[k, 0], r_one.at[k, 0], "fs", at.fx))
+        plane = at.twin(depth - 1 - k)
         pair_b = go(send(term_b.at[plane, 1 - at.y], one_b.at[k], s_one.at[k, 1], r_one.at[k, 1], "fs", at.fy))
-        first_stage.append((pair_a, pair_b))
+        first_stage.append((first_a_stage[k], pair_b))
     second_stage = []
     third_stage = []
     for k in range(depth + 1):
         if k < depth:
-            plane = at.plane(k + 1)
+            plane = at.twin(depth - 1 - k)
             first_stage[k][0].wait_recv()
             sum_a[k] = term_a[plane, :, at.x] + one_a[k]
             ca = go(send(sum_a.at[k, 1 - at.y], two_a.at[k], s_two.at[k, 0], r_two.at[k, 0], "fs", at.fy))
@@ -230,7 +317,7 @@
             second_stage.append((ca, cb))
         if k > 0:
             j = k - 1
-            target = at.plane(k) * PLANE + at.spot
+            target = at.twin(depth - k) * PLANE + at.spot
             second_stage[j][0].wait_recv()
             ready_a[j] = sum_a[j, at.y] + two_a[j]
             if j < depth - 1:
@@ -287,14 +374,52 @@
     scale = lax.rsqrt(joint / count + mean_floor)
     new_step = step_a[...] * scale[0:1, 0:1]
     step_a[...] = new_step
+    loads[3].wait()
     copy_a[at.f] = (master_a[...] - step_size * new_step).astype(jnp.bfloat16)
     new_step = step_b[...] * scale[8:9, 0:1]
     step_b[...] = new_step
+    loads[4].wait()
     copy_b[at.f] = (master_b[...] - step_size * new_step).astype(jnp.bfloat16)
 
-    gather(at, copy_a, copy_b, cz_s, cz_r, cp_s, cp_r)
+    stores = []
+
+    def put(base):
+        k = len(stores)
+        block = pl.ds(base, PLANE)
+        for side, (src, dst) in enumerate(((copy_a, copy_a_hbm), (copy_b, copy_b_hbm))):
+            stores.append(pltpu.make_async_copy(src.at[block], dst.at[block], store_sem.at[k + side]))
+            stores[-1].start()
+
+    gather(at, copy_a, copy_b, cz_s, cz_r, cp_s, cp_r, whole_block, put)
+    for store in stores:
+        store.wait()
     for copy in started:
         copy.wait_send()
+
+
+def hand_kernel(depth, *refs):
+    count = (len(refs) - 2) // 3
+    given, out, held = refs[:count], refs[count : 2 * count], refs[2 * count : 3 * count]
+    in_sem, out_sem = refs[3 * count :]
+    moves = []
+    for k in range(count):
+        pieces = depth if len(given[k].shape) == 3 else 1
+        size = given[k].shape[0] // pieces
+        for i in range(pieces):
+            part = pl.ds(i * size, size)
+            moves.append(
+                (
+                    pltpu.make_async_copy(given[k].at[part], held[k].at[part], in_sem.at[k, i]),
+                    pltpu.make_async_copy(held[k].at[part], out[k].at[part], out_sem.at[k, i]),
+                )
+            )
+    for into, _ in moves:
+        into.start()
+    for into, onward in moves:
+        into.wait()
+        onward.start()
+    for _, onward in moves:
+        onward.wait()
 
 
 def local(
@@ -313,40 +438,37 @@
     gate_second,
 ):
     in_vmem = pl.BlockSpec(memory_space=VMEM)
+    anywhere = pl.BlockSpec(memory_space=pl.ANY)
     rows, rank = input_factor.shape
+    tokens = saved_inputs.shape[0]
     low_rows, cols = input_first.shape
     depth = n // PLANE
     shape = jax.ShapeDtypeStruct
     f32, bf16 = jnp.float32, jnp.bfloat16
-    whole_in, whole_gate = pl.pallas_call(
-        functools.partial(factor_kernel, n),
-        out_shape=[shape((n, rows, rank), bf16)] * 2,
-        in_specs=[in_vmem] * 2,
-        out_specs=[in_vmem] * 2,
-        scratch_shapes=gather_sems(n),
-        compiler_params=pltpu.CompilerParams(collective_id=0, has_side_effects=True),
-        name="factors",
-    )(input_factor, gate_factor)
-
-    def term(whole, cot):
-        mid = jnp.dot(saved_inputs, whole.reshape(n * rows, rank), preferred_element_type=f32)
-        low = lax.dot_general(
-            mid, cot.astype(f32), (((0,), (0,)), ((), ())), precision=lax.Precision.HIGHEST
-        )
-        return low.reshape(depth, 2, 2, low_rows, cols)
-
-    term_in = term(whole_in, input_cot)
-    term_gate = term(whole_gate, gate_cot)
     low = shape((low_rows, cols), f32)
     piece = (low_rows, cols)
     full = shape((rows, cols), f32)
     copies = shape((n, rows, cols), bf16)
+    shapes = [full, full, low, low, low, low, copies, copies]
     outs = pl.pallas_call(
         functools.partial(main_kernel, n, m),
-        out_shape=[full, full, low, low, low, low, copies, copies],
-        in_specs=[in_vmem] * 10,
-        out_specs=[in_vmem] * 8,
+        out_shape=shapes,
+        in_specs=[anywhere] * 5 + [in_vmem] * 6,
+        out_specs=[in_vmem] * 6 + [anywhere] * 2,
         scratch_shapes=[
+            VMEM(saved_inputs.shape, bf16),
+            VMEM(input_cot.shape, bf16),
+            VMEM(input_cot.shape, bf16),
+            VMEM((rows, cols), f32),
+            VMEM((rows, cols), f32),
+            VMEM((n, rows, rank), bf16),
+            VMEM((n, rows, rank), bf16),
+            VMEM((tokens, rank), f32),
+            VMEM((tokens, rank), f32),
+            VMEM((depth, 2, 2) + piece, f32),
+            VMEM((depth, 2, 2) + piece, f32),
+            VMEM((n, rows, cols), bf16),
+            VMEM((n, rows, cols), bf16),
             VMEM((depth, 2) + piece, f32),
             VMEM((depth, 2) + piece, f32),
             VMEM((depth,) + piece, f32),
@@ -361,12 +483,10 @@
             VMEM((n,) + piece, f32),
             VMEM((m, 16, 128), f32),
             VMEM((n, 16, 128), f32),
-            DMA((depth, 2)),
-            DMA((depth, 2)),
-            DMA((depth, 2)),
-            DMA((depth, 2)),
-            DMA((depth, 2)),
-            DMA((depth, 2)),
+            DMA((5,)),
+            DMA((2 * depth,)),
+            *[DMA((depth, 2))] * 8,
+            *gather_sems(n),
             *gather_sems(n),
             DMA((m,)),
             DMA((m,)),
@@ -379,17 +499,26 @@
         ),
         name="update",
     )(
-        term_in,
-        term_gate,
+        saved_inputs,
+        input_cot,
+        gate_cot,
+        input_master,
+        gate_master,
+        input_factor,
+        gate_factor,
         input_first,
         input_second,
         gate_first,
         gate_second,
-        input_factor,
-        gate_factor,
-        input_master,
-        gate_master,
     )
+    outs = pl.pallas_call(
+        functools.partial(hand_kernel, depth),
+        out_shape=shapes,
+        in_specs=[anywhere] * 8,
+        out_specs=[anywhere] * 8,
+        scratch_shapes=[VMEM(s.shape, s.dtype) for s in shapes] + [DMA((8, depth))] * 2,
+        name="results",
+    )(*outs)
     *head, copy_in, copy_gate = outs
     return (*head, copy_in.reshape(n * rows, cols), copy_gate.reshape(n * rows, cols))
 

time: 201 us -> 176 us (0.88)
  the two profiles are of different devices: /device:TPU:24 before, /device:TPU:0 now
where the time goes in v2:
time: 176 us
  Pallas kernels  175 us (99%)
    pallas_call x1, Pallas kernels, local(): pl.pallas_call(functools.partial(main_kernel, n, m), out_shape=shapes, in...  167 us
    pallas_call x1, Pallas kernels, local(): pl.pallas_call(functools.partial(hand_kernel, depth), out_shape=shapes, i...  8.11 us

profile of v2, /device:TPU:0, one launch (start us, length us, event | category | flops | bytes accessed | tf_op | source)
XLA Modules:
  0.0 175.7 jit_solution(7269117533665001289)
XLA Ops:
  0.6 166.9 %update.1 = (f32[128,1024]{1,0:T(8,128)}, f32[128,1024]{1,0:T(8,128)}, f32[16,1024]{1,0:T(8,128)}, f32[16,1024]{1,0:T(8,128)}, f32[16,1024]{1,0:T(8,128)}, /*ind...) custom-call(bf16[768,2048]{1,0:T(8,128)(2,1)} %saved_hbm.1, ...), custom_call_target="tpu_custom_call" | custom-call | tf_op jit(solution)/shard_map/update/pallas_call | solution.py:453
  167.5 8.1 %results.1 = (f32[128,1024]{1,0:T(8,128)}, f32[128,1024]{1,0:T(8,128)}, f32[16,1024]{1,0:T(8,128)}, f32[16,1024]{1,0:T(8,128)}, f32[16,1024]{1,0:T(8,128)}, /*in...) custom-call(f32[128,1024]{1,0:T(8,128)} %get-tuple-element.24.refs_0_, ...), custom_call_target="tpu_custom_call" | custom-call | tf_op jit(solution)/shard_map/results/pallas_call | solution.py:514

commit v3 on v2

--- a/solution.py
+++ b/solution.py
@@ -100,6 +100,16 @@
         if s == 0:
             for dz in range(1, depth):
                 reach(dz)
+        if s == 1:
+            near[0][3].wait_recv()
+            near[0][4].wait_recv()
+            corner = at.z * PLANE + PLANE - 1 - at.spot
+            target = at.twin(1) * PLANE + at.spot
+            ca = go(a, corner, s_p.at[s, 4], r_p.at[s, 4], target)
+            cb = go(b, corner, s_p.at[s, 5], r_p.at[s, 5], target)
+            near[0] = near[0][:3]
+            near.append((base, xa, ya, yb, xb, ca, cb))
+            continue
         xa.wait_recv()
         ra = go(a, base + at.sx, s_p.at[s, 4], r_p.at[s, 4], at.fy)
         yb.wait_recv()

time: 176 us -> 167 us (0.949)
  Pallas kernels: 175 us -> 166 us
    pallas_call x1, Pallas kernels: 167 us -> 158 us  [local(): pl.pallas_call(functools.partial(main_kernel, n, m), out_shape=shapes, in...]
where the time goes in v3:
time: 167 us
  Pallas kernels  166 us (99%)
    pallas_call x1, Pallas kernels, local(): pl.pallas_call(functools.partial(main_kernel, n, m), out_shape=shapes, in...  158 us
    pallas_call x1, Pallas kernels, local(): pl.pallas_call(functools.partial(hand_kernel, depth), out_shape=shapes, i...  8.11 us

profile of v3, /device:TPU:0, one launch (start us, length us, event | category | flops | bytes accessed | tf_op | source)
XLA Modules:
  0.0 167.1 jit_solution(11092235093708117870)
XLA Ops:
  0.6 158.4 %update.1 = (f32[128,1024]{1,0:T(8,128)}, f32[128,1024]{1,0:T(8,128)}, f32[16,1024]{1,0:T(8,128)}, f32[16,1024]{1,0:T(8,128)}, f32[16,1024]{1,0:T(8,128)}, /*ind...) custom-call(bf16[768,2048]{1,0:T(8,128)(2,1)} %saved_hbm.1, ...), custom_call_target="tpu_custom_call" | custom-call | tf_op jit(solution)/shard_map/update/pallas_call | solution.py:463
  159.0 8.1 %results.1 = (f32[128,1024]{1,0:T(8,128)}, f32[128,1024]{1,0:T(8,128)}, f32[16,1024]{1,0:T(8,128)}, f32[16,1024]{1,0:T(8,128)}, f32[16,1024]{1,0:T(8,128)}, /*in...) custom-call(f32[128,1024]{1,0:T(8,128)} %get-tuple-element.24.refs_0_, ...), custom_call_target="tpu_custom_call" | custom-call | tf_op jit(solution)/shard_map/results/pallas_call | solution.py:524
